TPU v7x, 32 devices: a whole 2x2x4 slice. The times are simulated.
32 devices in a mesh: grp: 2 (over x), ep: 8 (over z, y), tp: 2 (over core).
Axes of the slice: x: 2, y: 2, z: 4, core: 2. Of those that a mesh axis runs over, the one named last changes fastest.
Arguments:
- tokens: bfloat16 [512, 2048], P(('grp', 'ep')), parts along dimension 0, may hold values from -6 to 6
- norm_gain: float32 [2048], replicated, may hold values from 0.1 to 1.9
- group_prob: float32 [512], P(('grp', 'ep')), parts along dimension 0, may hold values from 0.5 to 1
- route_logits: float32 [512, 4], P(('grp', 'ep')), parts along dimension 0, may hold values from -6 to 6
- expert_ids: int32 [512, 4], P(('grp', 'ep')), parts along dimension 0, may hold values from 0 to 7, as said below
- w_gate: bfloat16 [8, 2048, 512], P('ep', None, 'tp'), may hold values from -0.125 to 0.125
- w_up: bfloat16 [8, 2048, 512], P('ep', None, 'tp'), may hold values from -0.125 to 0.125
- w_down: bfloat16 [8, 512, 2048], P('ep', 'tp'), may hold values from -0.25 to 0.25
Outputs:
- mixed: bfloat16 [512, 2048], P(('grp', 'ep')), parts along dimension 0
There are 2 independent parts, one for each index of `grp`. A program takes and returns all parts, laid end to end along the dimension named above; an argument that names none is the same for every part. Nothing has to cross between parts.
Inputs may be any that keep to these rules, and one draw needn't show every extreme that they name: `expert_ids`: each token names 4 different experts, all inside one group of 4 consecutive experts. Of the 32 tokens of one index of ep, exactly 16 lie in each group, so at most 16 of them name any one expert; in every draw some expert is named by 16 tokens of every index of ep.
All inputs are finite; a program needn't handle non-finite values.
Results may differ from a plain program's by a relative error of at most 0.0077.
Values may be sent and summed in bfloat16 or wider, within the bound.
A program may use at most 64 MiB of HBM per device.

v0:
```python
import jax
import jax.numpy as jnp
from jax import lax
from jax.sharding import PartitionSpec as P

GROUPS = 2


def expert_rows(rows, w_gate, w_up, w_down):
    gate = jnp.dot(rows, w_gate[0], preferred_element_type=jnp.float32)
    up = jnp.dot(rows, w_up[0], preferred_element_type=jnp.float32)
    act = (jax.nn.silu(gate) * up).astype(jnp.bfloat16)
    part = jnp.dot(act, w_down[0], preferred_element_type=jnp.float32).astype(jnp.bfloat16)
    return lax.optimization_barrier(part).astype(jnp.float32)


def shards(tokens, norm_gain, group_prob, route_logits, expert_ids, w_gate, w_up, w_down):
    values = tokens.astype(jnp.float32)
    scale = lax.rsqrt(jnp.mean(values * values, axis=-1, keepdims=True) + 1e-06)
    normed = (values * scale * norm_gain).astype(jnp.bfloat16)
    expw = jnp.exp(route_logits)
    route_w = group_prob[:, None] * expw / jnp.sum(expw, axis=-1, keepdims=True)
    width = lax.axis_size("ep")
    count = tokens.shape[0]
    topk = expert_ids.shape[1]
    dmodel = tokens.shape[1]
    capacity = count // GROUPS
    pairs = expert_ids.reshape(-1)
    onehot = (pairs[:, None] == jnp.arange(width, dtype=jnp.int32)[None, :]).astype(jnp.int32)
    before = jnp.cumsum(onehot, axis=0) - onehot
    position = jnp.sum(onehot * before, axis=1)
    slot = pairs * capacity + position
    place = (slot[:, None] == jnp.arange(width * capacity, dtype=jnp.int32)[None, :]).astype(
        jnp.bfloat16
    )
    spread = jnp.repeat(normed, topk, axis=0)
    send = lax.dot_general(
        place, spread, (((0,), (0,)), ((), ())), preferred_element_type=jnp.float32
    )
    send = send.astype(jnp.bfloat16).reshape(width, capacity, dmodel)
    received = lax.all_to_all(send, "ep", split_axis=0, concat_axis=0, tiled=True)
    slots = received.shape[1]
    part = expert_rows(received.reshape(-1, dmodel), w_gate, w_up, w_down)
    total = lax.psum_scatter(part.astype(jnp.bfloat16), "tp", scatter_dimension=1, tiled=True)
    served = total.reshape(width, slots, total.shape[1])
    back = lax.all_to_all(served, "ep", split_axis=0, concat_axis=0, tiled=True)
    chosen = jnp.take(back.reshape(-1, back.shape[2]), slot, axis=0)
    picked = lax.all_gather(chosen, "tp", axis=1, tiled=True)
    weighted = picked.astype(jnp.float32).reshape(count, topk, dmodel) * route_w[:, :, None]
    return jnp.sum(weighted, axis=1).astype(jnp.bfloat16)


def solution(mesh):
    in_specs = (
        P(("grp", "ep"), None),
        P(),
        P(("grp", "ep")),
        P(("grp", "ep"), None),
        P(("grp", "ep"), None),
        P("ep", None, "tp"),
        P("ep", None, "tp"),
        P("ep", "tp", None),
    )
    out_specs = P(("grp", "ep"), None)
    return jax.shard_map(shards, mesh=mesh, in_specs=in_specs, out_specs=out_specs, check_vma=False)
```

profile of v0, /device:TPU:0, one launch (start us, length us, event | category | flops | bytes accessed | tf_op | source)
XLA Modules:
  0.0 68.6 jit_solution(7120722559615207689)
XLA Ops:
  6.5 0.0 copy-start
  6.5 0.0 reduce-scatter.2.cloned.1.call-start
  6.5 0.8 %copy.12 = s32[32,4]{1,0:T(8,128)S(1)} copy(s32[32,4]{0,1:T(4,128)} %param.12) | data formatting | bytes 1024 | tf_op args[4]
  7.4 0.1 reshape.77
  7.5 0.0 copy-start.3
  7.5 0.1 fusion.15
  7.6 0.2 reduce_window_sum.11
  7.8 0.2 select_reduce_fusion
  8.0 0.4 copy-done.3
  8.4 0.0 copy-start.4
  8.4 0.1 fusion.6
  8.6 0.5 copy-done.4
  9.1 0.1 fusion.8
  9.2 0.2 broadcast_in_dim.10
  9.4 0.1 reshape.78
  9.6 0.0 copy-start.2
  9.6 0.4 convolution_convert_fusion.1
  10.0 21.6 %all_to_all.10 = bf16[8,16,2048]{2,1,0:T(8,128)(2,1)S(1)} all-to-all(bf16[8,16,2048]{2,1,0:T(8,128)(2,1)S(1)} %bitcast.26), channel_id=1, replica_groups=mesh['grp'=2,'ep'=8,'tp'=2] {'ep'}, dimensions={0} | all-to-all | bytes 1048576 | tf_op jit(solution)/shard_map/all_to_all | solution.py:41
  31.6 0.0 copy-start.1
  31.6 0.0 copy-done.2
  31.6 0.3 fusion.4
  32.0 0.0 copy-done
  32.0 0.9 %copy-done.1 = bf16[1,2048,256]{2,1,0:T(8,128)(2,1)S(1)} copy-done((bf16[1,2048,256]{2,1,0:T(8,128)(2,1)S(1)}, bf16[1,2048,256]{2,1,0:T(8,128)(2,1)}, u32[]{:S(2)}) %copy-start.1) | copy-done | bytes 1048600
  32.9 1.6 %convolution_convert_fusion = bf16[128,2048]{1,0:T(8,128)(2,1)} fusion(bf16[128,2048]{1,0:T(8,128)(2,1)S(1)} %bitcast.25, bf16[1,256,2048]{2,1,0:T(8,128)(2,1)S(1)} %copy-done, bf16[1,2048,256]{2,1,0:T(8,128)(2,1)S(1)} %copy-done.1, f32[128,256]{1,0:T(8,128)S(1)} %fusion.4), kind=kOutput, calls=%fused_computation.1 | convolution fusion | flops 268894208 | bytes 3276800 | tf_op jit(solution)/shard_map/dot_general | solution.py:13
  34.4 0.0 copy-start.5
  34.4 0.0 reduce-scatter.2.cloned.1.call-update
  34.5 0.7 copy-done.5
  35.1 0.1 copy.13
  35.2 0.0 copy-start.6
  35.2 0.1 mul.82
  35.3 0.6 copy-done.6
  35.9 5.6 %reduce-scatter.2.cloned.1.call-done = bf16[128,1024]{1,0:T(8,128)(2,1)} async-done(((bf16[128,2048]{1,0:T(8,128)(2,1)}), bf16[128,1024]{1,0:T(8,128)(2,1)}) %reduce-scatter.2.cloned.1.call-update) | async-done | bytes 262160 | tf_op jit(solution)/shard_map/reduce_scatter | solution.py:44
  41.6 0.0 copy-start.7
  41.6 5.9 %all-to-all-start.1 = ((bf16[8,16,1024]{2,1,0:T(8,128)(2,1)}), bf16[8,16,1024]{2,1,0:T(8,128)(2,1)S(1)}, u32[]{:S(2)}, u32[]{:S(2)}) async-start(bf16[8,16,1024]{2,1,0:T(8,128)(2,1)} %bitcast.27), calls=%async_computation.2 | async-start | bytes 524288 | tf_op jit(solution)/shard_map/all_to_all | solution.py:46
  47.4 0.0 copy-done.7
  47.4 0.1 copy.14
  47.5 9.3 %all-to-all-done.1 = bf16[8,16,1024]{2,1,0:T(8,128)(2,1)S(1)} async-done(((bf16[8,16,1024]{2,1,0:T(8,128)(2,1)}), bf16[8,16,1024]{2,1,0:T(8,128)(2,1)S(1)}, u32[]{:S(2)}, u32[]{:S(2)}) %all-to-all-start.1) | async-done | bytes 262176 | tf_op jit(solution)/shard_map/all_to_all | solution.py:46
  56.9 0.9 %gather_fusion = bf16[128,1024]{1,0:T(8,128)(2,1)S(1)} fusion(bf16[128,1024]{1,0:T(8,128)(2,1)S(1)} %bitcast.23, s32[1024]{0:T(1024)S(1)} %pad_clamp_fusion), kind=kCustom, calls=%fused_computation | custom fusion | bytes 524800 | tf_op jit(solution)/shard_map/jit(_take)/gather | solution.py:47
  57.7 0.1 broadcast_select_fusion
  57.8 2.2 %all_gather.3 = bf16[128,2048]{1,0:T(8,128)(2,1)S(1)} all-gather(bf16[128,1024]{1,0:T(8,128)(2,1)S(1)} %broadcast_select_fusion), channel_id=1, replica_groups=mesh['grp'=2,'ep'=8,'tp'=2] {'tp'}, dimensions={1}, use_global_device_ids=true | all-gather | bytes 786432 | tf_op jit(solution)/shard_map/all_gather | solution.py:48
  60.0 0.3 reshape.86
  60.3 1.4 %multiply_reduce_fusion = bf16[32,2048]{1,0:T(8,128)(2,1)} fusion(f32[32,4,2048]{2,1,0:T(4,128)S(1)} %reshape.86, f32[32,4]{1,0:T(8,128)S(1)} %copy.14), kind=kLoop, calls=%fused_computation.9 | loop fusion | flops 458752 | bytes 1180160 | tf_op jit(solution)/shard_map/reduce_sum | solution.py:50
  (7 shorter events, 0.1 us)
Async XLA Ops:
  6.5 25.4 %copy-start = (bf16[1,256,2048]{2,1,0:T(8,128)(2,1)S(1)}, bf16[1,256,2048]{2,1,0:T(8,128)(2,1)}, u32[]{:S(2)}) copy-start(bf16[1,256,2048]{2,1,0:T(8,128)(2,1)} %param.15) | copy-start | bytes 3145732
  6.5 35.0 %reduce-scatter.2.cloned.1.call-start = ((), (), s32[]{:S(2)}) async-start(), calls=%async_computation.3 | async-start | bytes 786432 | tf_op jit(solution)/shard_map/reduce_scatter | solution.py:44
  7.5 0.9 %copy-start.3 = (bf16[32,2048]{1,0:T(8,128)(2,1)S(1)}, bf16[32,2048]{1,0:T(8,128)(2,1)}, u32[]{:S(2)}) copy-start(bf16[32,2048]{1,0:T(8,128)(2,1)} %param.8) | copy-start | bytes 393220
  8.4 0.7 %copy-start.4 = (f32[2048]{0:T(1024)S(1)}, f32[2048]{0:T(1024)}, u32[]{:S(2)}) copy-start(f32[2048]{0:T(1024)} %param.9) | copy-start | bytes 24580
  9.6 22.1 %copy-start.2 = (bf16[1,2048,256]{2,1,0:T(8,128)(2,1)S(1)}, bf16[1,2048,256]{2,1,0:T(8,128)(2,1)}, u32[]{:S(2)}) copy-start(bf16[1,2048,256]{2,1,0:T(8,128)(2,1)} %param.13) | copy-start | bytes 3145732
  31.6 1.2 %copy-start.1 = (bf16[1,2048,256]{2,1,0:T(8,128)(2,1)S(1)}, bf16[1,2048,256]{2,1,0:T(8,128)(2,1)}, u32[]{:S(2)}) copy-start(bf16[1,2048,256]{2,1,0:T(8,128)(2,1)} %param.14) | copy-start | bytes 3145732
  34.4 0.7 copy-start.5
  35.2 0.7 copy-start.6
  41.6 5.9 %copy-start.7 = (f32[32]{0:T(128)S(1)}, f32[32]{0:T(128)}, u32[]{:S(2)}) copy-start(f32[32]{0:T(128)} %param.10) | copy-start | bytes 388
  41.6 15.3 %all-to-all-start.1 = ((bf16[8,16,1024]{2,1,0:T(8,128)(2,1)}), bf16[8,16,1024]{2,1,0:T(8,128)(2,1)S(1)}, u32[]{:S(2)}, u32[]{:S(2)}) async-start(bf16[8,16,1024]{2,1,0:T(8,128)(2,1)} %bitcast.27), calls=%async_computation.2 | async-start | bytes 524288 | tf_op jit(solution)/shard_map/all_to_all | solution.py:46
Sparse Core Ops, SparseCore 0:
  34.6 6.9 reduce-scatter.1
where the time goes:
time: 69 us; the launch traced here: 68.6 us
  blocking collectives  23.8 us (34%)
  waiting for transfers between devices  15 us (22%)
  between operations  13.5 us (20%)
  local copies, waits for them, and re-layouts  5.91 us (9%)
  starting transfers between devices  5.86 us (8%)
  matrix products  2.29 us (3%)
  other arithmetic  2.21 us (3%)
    all_to_all x1, blocking collectives, shards(): lax.all_to_all(send, 'ep', split_axis=0, concat_axis=0, tiled=True)  21.6 us
    all_to_all x1, waiting for transfers between devices, shards(): back = lax.all_to_all(served, 'ep', split_axis=0, concat_axis=0, tiled=True)  9.32 us
    all_to_all x1, starting transfers between devices, shards(): back = lax.all_to_all(served, 'ep', split_axis=0, concat_axis=0, tiled=True)  5.85 us
    reduce_scatter x1, waiting for transfers between devices, shards(): lax.psum_scatter(part.astype(jnp.bfloat16), 'tp', scatter_dimension=1, ti...  5.64 us
    unnamed x17, local copies, waits for them, and re-layouts  3.98 us
    all_gather x1, blocking collectives, shards(): picked = lax.all_gather(chosen, 'tp', axis=1, tiled=True)  2.18 us
    dot_general x1, matrix products, expert_rows(): jnp.dot(act, w_down[0], preferred_element_type=jnp.float32)  1.57 us
    reduce_sum x1, other arithmetic, shards(): return jnp.sum(weighted, axis=1).astype(jnp.bfloat16)  1.4 us
  transfers between devices with their start and end apart: 2, of which 2 were waited for; matrix products, arithmetic and copies ran while one was open for 0% of the time, Pallas kernels for 0%

commit v1 on v0

v1 whole, which is shorter than its diff:
```python
import functools

import jax
import jax.numpy as jnp
from jax import lax
from jax.experimental import pallas as pl
from jax.experimental.pallas import tpu as pltpu
from jax.sharding import PartitionSpec as P

GROUPS = 2
MESH = pl.DeviceIdType.MESH


def kernel(
    width, n_tp,
    tok_hbm, gain_hbm, prob_hbm, logit_hbm, ids_hbm, wg_hbm, wu_hbm, wd_hbm,
    out_ref,
    tok, gain, prob, logit, ids, wg, wu, wd, send, recv, outs, back, mixed,
    in_sem, wl_sem, ws_sem, wr_sem, ds_sem, dr_sem, bs_sem, br_sem, ms_sem, mr_sem,
):
    e = lax.axis_index("ep")
    q = lax.axis_index("tp")
    sib = n_tp - 1 - q
    gs = width // GROUPS
    nsrc = width // n_tp
    hb = nsrc // GROUPS
    count, dmodel = tok.shape
    cap = count // GROUPS
    topk = ids.shape[0]
    block = e // gs
    mine = (block == q) & (e % n_tp == q)

    smalls = [
        pltpu.make_async_copy(src, dst, in_sem.at[i])
        for i, (src, dst) in enumerate(
            [(tok_hbm, tok), (gain_hbm, gain), (prob_hbm, prob), (logit_hbm, logit), (ids_hbm, ids)]
        )
    ]
    for c in smalls:
        c.start()
    weights = [(wg_hbm, wg), (wu_hbm, wu), (wd_hbm, wd)]
    locals_ = [
        pltpu.make_async_copy(src.at[0], dst.at[q], wl_sem.at[i]) for i, (src, dst) in enumerate(weights)
    ]
    for c in locals_:
        c.start()

    barrier = pltpu.get_barrier_semaphore()
    pl.semaphore_signal(barrier, inc=1, device_id={"tp": sib}, device_id_type=MESH)
    for j in range(gs):
        dest = q * gs + j

        @pl.when(jnp.logical_not(mine & (dest == e)))
        def _():
            pl.semaphore_signal(
                barrier, inc=1, device_id={"ep": dest, "tp": e % n_tp}, device_id_type=MESH
            )

    for i in range(nsrc):
        src = i * n_tp + q

        @pl.when(jnp.logical_not(mine & (src == e)))
        def _():
            pl.semaphore_signal(
                barrier, inc=1, device_id={"ep": src, "tp": block}, device_id_type=MESH
            )

    for c in smalls:
        c.wait()
    values = tok[...].astype(jnp.float32)
    scale = lax.rsqrt(jnp.mean(values * values, axis=-1, keepdims=True) + 1e-06)
    normed = (values * scale * gain[...]).astype(jnp.bfloat16)
    idv = ids[...]
    first = idv[0:1, :]
    grow = jnp.zeros((1, count), jnp.float32)
    for g in range(1, GROUPS):
        grow = grow + jnp.where(first >= g * gs, 1.0, 0.0)
    t_row = lax.broadcasted_iota(jnp.int32, (count, count), 0)
    t_col = lax.broadcasted_iota(jnp.int32, (count, count), 1)
    gfull = jnp.broadcast_to(grow, (count, count))
    gcol = jnp.sum(jnp.where(t_row == t_col, gfull, 0.0), axis=1, keepdims=True)
    same = jnp.where(gfull == gcol, 1.0, 0.0)
    pos_row = jnp.sum(jnp.where(t_row < t_col, same, 0.0), axis=0, keepdims=True)
    pos_col = jnp.sum(jnp.where(t_col < t_row, same, 0.0), axis=1, keepdims=True)
    qf = q.astype(jnp.float32)
    r_io = lax.broadcasted_iota(jnp.int32, (cap, count), 0).astype(jnp.float32)
    place = jnp.where((pos_row == r_io) & (grow == qf), 1.0, 0.0)
    send[...] = jnp.dot(
        place.astype(jnp.bfloat16), normed, preferred_element_type=jnp.float32
    ).astype(jnp.bfloat16)

    @pl.when(mine)
    def _():
        recv[e // n_tp] = send[...]

    wait_n = jnp.where(mine, gs + nsrc - 1, gs + nsrc + 1)
    pl.semaphore_wait(barrier, wait_n)

    def dispatch(j):
        dest = q * gs + j
        return dest, pltpu.make_async_remote_copy(
            src_ref=send,
            dst_ref=recv.at[e // n_tp],
            send_sem=ds_sem.at[j],
            recv_sem=dr_sem.at[e // n_tp],
            device_id={"ep": dest, "tp": e % n_tp},
            device_id_type=MESH,
        )

    for j in range(gs):
        dest, copy = dispatch(j)

        @pl.when(jnp.logical_not(mine & (dest == e)))
        def _():
            copy.start()

    swaps = [
        pltpu.make_async_remote_copy(
            src_ref=src.at[0],
            dst_ref=dst.at[q],
            send_sem=ws_sem.at[i],
            recv_sem=wr_sem.at[i],
            device_id={"tp": sib},
            device_id_type=MESH,
        )
        for i, (src, dst) in enumerate(weights)
    ]
    for c in swaps:
        c.start()

    expw = jnp.exp(logit[...])
    route = prob[...] * expw / jnp.sum(expw, axis=0, keepdims=True)
    expert = lax.broadcasted_iota(jnp.int32, (128, count), 0) + q * gs
    wtok = jnp.zeros((128, count), jnp.float32)
    for k in range(topk):
        wtok = wtok + jnp.where(idv[k : k + 1, :] == expert, route[k : k + 1, :], 0.0)
    wslot = lax.dot_general(
        place, wtok, (((1,), (1,)), ((), ())),
        precision=lax.Precision.HIGHEST, preferred_element_type=jnp.float32,
    )
    s_io = lax.broadcasted_iota(jnp.int32, (count, count), 1).astype(jnp.float32)
    unplace = jnp.where(s_io == gcol * cap + pos_col, 1.0, 0.0).astype(jnp.bfloat16)

    def give(i):
        home = i * n_tp + q
        return home, pltpu.make_async_remote_copy(
            src_ref=outs.at[i],
            dst_ref=back.at[e % gs],
            send_sem=bs_sem.at[i],
            recv_sem=br_sem.at[e % gs],
            device_id={"ep": home, "tp": block},
            device_id_type=MESH,
        )

    for c in locals_:
        c.wait()
    for step in range(GROUPS):
        b = lax.rem(block + step, GROUPS)
        for i in range(hb):
            slot = b * hb + i

            @pl.when(jnp.logical_not(mine & (slot * n_tp + q == e)))
            def _():
                pltpu.make_async_remote_copy(
                    src_ref=send,
                    dst_ref=recv.at[slot],
                    send_sem=ds_sem.at[0],
                    recv_sem=dr_sem.at[slot],
                    device_id={"tp": sib},
                    device_id_type=MESH,
                ).wait_recv()

        def arrived(i):
            if step == 0:
                src, dst = weights[i]
                pltpu.make_async_remote_copy(
                    src_ref=src.at[0],
                    dst_ref=dst.at[sib],
                    send_sem=ws_sem.at[i],
                    recv_sem=wr_sem.at[i],
                    device_id={"tp": sib},
                    device_id_type=MESH,
                ).wait_recv()

        x = recv[pl.ds(b * hb, hb)].reshape(hb * cap, dmodel)
        arrived(0)
        gates = [jnp.dot(x, wg[h], preferred_element_type=jnp.float32) for h in range(n_tp)]
        arrived(1)
        ups = [jnp.dot(x, wu[h], preferred_element_type=jnp.float32) for h in range(n_tp)]
        acts = [((g / (1.0 + jnp.exp(-g))) * u).astype(jnp.bfloat16) for g, u in zip(gates, ups)]
        arrived(2)
        total = jnp.dot(acts[0], wd[0], preferred_element_type=jnp.float32)
        for h in range(1, n_tp):
            total = total + jnp.dot(acts[h], wd[h], preferred_element_type=jnp.float32)
        outs[pl.ds(b * hb, hb)] = total.astype(jnp.bfloat16).reshape(hb, cap, dmodel)
        for i in range(hb):
            slot = b * hb + i
            home, copy = give(slot)

            @pl.when(jnp.logical_not(mine & (home == e)))
            def _():
                copy.start()

            @pl.when(mine & (home == e))
            def _():
                back[e % gs] = outs[slot]

    acc = jnp.zeros((cap, dmodel), jnp.float32)
    for j in range(gs):

        @pl.when(jnp.logical_not(mine & (q * gs + j == e)))
        def _():
            pltpu.make_async_remote_copy(
                src_ref=outs.at[0],
                dst_ref=back.at[j],
                send_sem=bs_sem.at[0],
                recv_sem=br_sem.at[j],
                device_id={"tp": sib},
                device_id_type=MESH,
            ).wait_recv()

        acc = acc + wslot[:, j : j + 1] * back[j].astype(jnp.float32)
    mixed[q] = acc.astype(jnp.bfloat16)
    swap = pltpu.make_async_remote_copy(
        src_ref=mixed.at[q],
        dst_ref=mixed.at[q],
        send_sem=ms_sem,
        recv_sem=mr_sem,
        device_id={"tp": sib},
        device_id_type=MESH,
    )
    swap.start()

    for j in range(gs):
        dest, copy = dispatch(j)

        @pl.when(jnp.logical_not(mine & (dest == e)))
        def _():
            copy.wait_send()

    for c in swaps:
        c.wait_send()
    for i in range(nsrc):
        home, copy = give(i)

        @pl.when(jnp.logical_not(mine & (home == e)))
        def _():
            copy.wait_send()

    pltpu.make_async_remote_copy(
        src_ref=mixed.at[q],
        dst_ref=mixed.at[sib],
        send_sem=ms_sem,
        recv_sem=mr_sem,
        device_id={"tp": sib},
        device_id_type=MESH,
    ).wait_recv()
    swap.wait_send()
    slots = mixed[...].reshape(count, dmodel)
    out_ref[...] = jnp.dot(unplace, slots, preferred_element_type=jnp.float32).astype(jnp.bfloat16)


def shards(tokens, norm_gain, group_prob, route_logits, expert_ids, w_gate, w_up, w_down):
    width = lax.axis_size("ep")
    n_tp = lax.axis_size("tp")
    count, dmodel = tokens.shape
    topk = expert_ids.shape[1]
    ff = w_gate.shape[2]
    cap = count // GROUPS
    gs = width // GROUPS
    nsrc = width // n_tp
    hbm = pl.BlockSpec(memory_space=pltpu.HBM)
    bf, f32 = jnp.bfloat16, jnp.float32
    dma = pltpu.SemaphoreType.DMA
    return pl.pallas_call(
        functools.partial(kernel, width, n_tp),
        out_shape=jax.ShapeDtypeStruct((count, dmodel), bf),
        in_specs=[hbm] * 8,
        out_specs=pl.BlockSpec(memory_space=pltpu.VMEM),
        scratch_shapes=[
            pltpu.VMEM((count, dmodel), bf),
            pltpu.VMEM((1, dmodel), f32),
            pltpu.VMEM((1, count), f32),
            pltpu.VMEM((topk, count), f32),
            pltpu.VMEM((topk, count), jnp.int32),
            pltpu.VMEM((n_tp, dmodel, ff), bf),
            pltpu.VMEM((n_tp, dmodel, ff), bf),
            pltpu.VMEM((n_tp, ff, dmodel), bf),
            pltpu.VMEM((cap, dmodel), bf),
            pltpu.VMEM((nsrc, cap, dmodel), bf),
            pltpu.VMEM((nsrc, cap, dmodel), bf),
            pltpu.VMEM((gs, cap, dmodel), bf),
            pltpu.VMEM((n_tp, cap, dmodel), bf),
            dma((5,)), dma((3,)), dma((3,)), dma((3,)),
            dma((gs,)), dma((nsrc,)), dma((nsrc,)), dma((gs,)),
            dma, dma,
        ],
        compiler_params=pltpu.CompilerParams(collective_id=0, has_side_effects=True),
        name="expert_mixture",
    )(
        tokens, norm_gain.reshape(1, dmodel), group_prob.reshape(1, count), route_logits.T,
        expert_ids.T, w_gate, w_up, w_down,
    )


def solution(mesh):
    in_specs = (
        P(("grp", "ep"), None),
        P(),
        P(("grp", "ep")),
        P(("grp", "ep"), None),
        P(("grp", "ep"), None),
        P("ep", None, "tp"),
        P("ep", None, "tp"),
        P("ep", "tp", None),
    )
    out_specs = P(("grp", "ep"), None)
    return jax.shard_map(shards, mesh=mesh, in_specs=in_specs, out_specs=out_specs, check_vma=False)
```

time: 69 us -> 23.7 us (0.34)
  blocking collectives: 23.8 us -> 0 us
  Pallas kernels: 0 us -> 22 us
  waiting for transfers between devices: 15 us -> 0 us
  between operations: 13.5 us -> 0.01 us
  starting transfers between devices: 5.86 us -> 0 us
  local copies, waits for them, and re-layouts: 5.91 us -> 1.57 us
  matrix products: 2.29 us -> 0 us
  other arithmetic: 2.21 us -> 0 us
    pallas_call x0 -> x1, Pallas kernels: none -> 22 us  [shards(): pl.pallas_call(functools.partial(kernel, width, n_tp), out_shape=jax.Shap...]
    all_to_all x1 -> x0, blocking collectives: 21.6 us -> none  [shards(): lax.all_to_all(send, 'ep', split_axis=0, concat_axis=0, tiled=True)]
    all_to_all x1 -> x0, waiting for transfers between devices: 9.32 us -> none  [shards(): back = lax.all_to_all(served, 'ep', split_axis=0, concat_axis=0, tiled=True)]
    all_to_all x1 -> x0, starting transfers between devices: 5.85 us -> none  [shards(): back = lax.all_to_all(served, 'ep', split_axis=0, concat_axis=0, tiled=True)]
    reduce_scatter x1 -> x0, waiting for transfers between devices: 5.64 us -> none  [shards(): lax.psum_scatter(part.astype(jnp.bfloat16), 'tp', scatter_dimension=1, ti...]
    unnamed x17 -> x1, local copies, waits for them, and re-layouts: 3.98 us -> 1.57 us
    dot_general x3 -> x0, matrix products: 2.29 us -> none  [the longest x1 1.57 us: expert_rows(): jnp.dot(act, w_down[0], preferred_element_type=jnp.float32)]
    all_gather x1 -> x0, blocking collectives: 2.18 us -> none  [shards(): picked = lax.all_gather(chosen, 'tp', axis=1, tiled=True)]
  transfers between devices with their start and end apart: 2 -> 0, of which waited for: 2 -> 0; matrix products, arithmetic and copies ran while one was open for 0% -> 0% of each run, Pallas kernels for 0% -> 0%
where the time goes in v1:
time: 23.7 us; the launch traced here: 23.6 us
  Pallas kernels  22 us (93%)
  local copies, waits for them, and re-layouts  1.57 us (7%)
    pallas_call x1, Pallas kernels, shards(): pl.pallas_call(functools.partial(kernel, width, n_tp), out_shape=jax.Shap...  22 us
    unnamed x1, local copies, waits for them, and re-layouts  1.57 us

profile of v1, /device:TPU:0, one launch (start us, length us, event | category | flops | bytes accessed | tf_op | source)
XLA Modules:
  0.0 23.6 jit_solution(15079887681769604756)
XLA Ops:
  0.0 22.0 %expert_mixture.1 = bf16[32,2048]{1,0:T(8,128)(2,1)} custom-call(bf16[32,2048]{1,0:T(8,128)(2,1)} %tok_hbm.1, f32[1,2048]{1,0:T(1,128)} %bitcast.4, f32[1,32]{1,0:T(1,128)} %bitcast.7, f32[4,32]{1,0:T(4,128)} %bitcast.5, s32[4,32]{1,0:T(4,128)} %bitcast.6, bf16[1,2048,256]{2,1,0:T(8,128)(2,1)} %wg_hbm.1, bf16[1,2048,256]{2,1,0:T(8,128)(2,1)} %wu_hbm.1, ...), custom_call_target="tpu_custom_call" | custom-call | tf_op jit(solution)/shard_map/expert_mixture/pallas_call | solution.py:275
  22.0 1.6 %copy.10 = bf16[32,2048]{1,0:T(8,128)(2,1)} copy(bf16[32,2048]{1,0:T(8,128)(2,1)} %expert_mixture.1) | data formatting | bytes 262144

commit v2 on v1

--- a/solution.py
+++ b/solution.py
@@ -274,7 +274,7 @@
     dma = pltpu.SemaphoreType.DMA
     return pl.pallas_call(
         functools.partial(kernel, width, n_tp),
-        out_shape=jax.ShapeDtypeStruct((count, dmodel), bf),
+        out_shape=pltpu.VMEM((count, dmodel), bf),
         in_specs=[hbm] * 8,
         out_specs=pl.BlockSpec(memory_space=pltpu.VMEM),
         scratch_shapes=[

time: 23.7 us -> 22.2 us (0.937)
  local copies, waits for them, and re-layouts: 1.57 us -> 0.66 us
  Pallas kernels: 22 us -> 21.4 us
    unnamed x1, local copies, waits for them, and re-layouts: 1.57 us -> 0.66 us
    pallas_call x1, Pallas kernels: 22 us -> 21.4 us  [shards(): pl.pallas_call(functools.partial(kernel, width, n_tp), out_shape=pltpu.VM...]
where the time goes in v2:
time: 22.2 us; the launch traced here: 22 us
  Pallas kernels  21.4 us (96%)
  local copies, waits for them, and re-layouts  0.66 us (3%)
    pallas_call x1, Pallas kernels, shards(): pl.pallas_call(functools.partial(kernel, width, n_tp), out_shape=pltpu.VM...  21.4 us
    unnamed x1, local copies, waits for them, and re-layouts  0.66 us

profile of v2, /device:TPU:0, one launch (start us, length us, event | category | flops | bytes accessed | tf_op | source)
XLA Modules:
  0.0 22.0 jit_solution(17251041690741424203)
XLA Ops:
  0.0 21.4 %expert_mixture.1 = bf16[32,2048]{1,0:T(8,128)(2,1)S(1)} custom-call(bf16[32,2048]{1,0:T(8,128)(2,1)} %tok_hbm.1, f32[1,2048]{1,0:T(1,128)} %bitcast.4, f32[1,32]{1,0:T(1,128)} %bitcast.7, f32[4,32]{1,0:T(4,128)} %bitcast.5, s32[4,32]{1,0:T(4,128)} %bitcast.6, bf16[1,2048,256]{2,1,0:T(8,128)(2,1)} %wg_hbm.1, bf16[1,2048,256]{2,1,0:T(8,128)(2,1)} %wu_hbm.1, ...), custom_call_target="tpu_custom_call" | custom-call | tf_op jit(solution)/shard_map/expert_mixture/pallas_call | solution.py:275
  21.4 0.7 %copy.10 = bf16[32,2048]{1,0:T(8,128)(2,1)} copy(bf16[32,2048]{1,0:T(8,128)(2,1)S(1)} %expert_mixture.1) | data formatting | bytes 262144
